TPU v7x, 32 devices: a whole 2x2x4 slice. The times are simulated.
32 devices in a mesh: grp: 2 (over y), sp: 4 (over z), dp: 4 (over x, core).
Axes of the slice: x: 2, y: 2, z: 4, core: 2. Of those that a mesh axis runs over, the one named last changes fastest.
Arguments:
- query_rows: bfloat16 [8, 512, 2048], P(('grp', 'dp'), 'sp'), parts along dimension 0, may hold values from -6 to 6
- key_rows: bfloat16 [8, 512, 2048], P(('grp', 'dp'), 'sp'), parts along dimension 0, may hold values from -6 to 6
- value_rows: bfloat16 [8, 512, 2048], P(('grp', 'dp'), 'sp'), parts along dimension 0, may hold values from -6 to 6
- query_gain: float32 [64], replicated, may hold values from 1.1 to 7
- key_gain: float32 [64], replicated, may hold values from 1.1 to 7
- lambdas: float32 [16], replicated, may hold values from 0.3 to 0.8
- head_gain: float32 [128], replicated, may hold values from 0.1 to 1.9
- out_weight: bfloat16 [2048, 2048], P(None, 'dp'), may hold values from -0.125 to 0.125
Outputs:
- attended: bfloat16 [8, 512, 2048], P(('grp', 'dp'), 'sp'), parts along dimension 0
There are 2 independent parts, one for each index of `grp`. A program takes and returns all parts, laid end to end along the dimension named above; an argument that names none is the same for every part. Nothing has to cross between parts.
All inputs are finite; a program needn't handle non-finite values.
Results may differ from a plain program's by a relative error of at most 0.008.
The roundings to bfloat16 on the way count: a program that leaves them out, or rounds other values in their place, can miss the bound.
Values may be sent and summed in bfloat16 or wider, within the bound.
A program may use at most 128 MiB of HBM per device.

v0:
```python
import jax
import jax.numpy as jnp
from jax import lax
from jax.sharding import PartitionSpec as P

EPSILON = 1e-06
OUT_SCALE = 0.8


def norm_rotate(field_rows, gain_vector, positions):
    widened = field_rows.astype(jnp.float32)
    normed = (
        widened
        * lax.rsqrt(jnp.mean(widened * widened, axis=-1, keepdims=True) + EPSILON)
        * gain_vector
    )
    half_size = field_rows.shape[-1] // 2
    inverse = 10000.0 ** (-jnp.arange(half_size, dtype=jnp.float32) / half_size)
    angles = (positions[:, None] * inverse[None, :]).reshape(positions.shape[0], 1, 1, half_size)
    cosine_part = jnp.cos(angles)
    sine_part = jnp.sin(angles)
    first_half = normed[..., :half_size]
    second_half = normed[..., half_size:]
    turned = jnp.concatenate(
        [
            first_half * cosine_part - second_half * sine_part,
            second_half * cosine_part + first_half * sine_part,
        ],
        axis=-1,
    )
    return turned.astype(jnp.bfloat16)


def head_norm(raw_heads, gain_vector):
    scaled = raw_heads * lax.rsqrt(
        jnp.mean(raw_heads * raw_heads, axis=-1, keepdims=True) + EPSILON
    )
    return (scaled * gain_vector * OUT_SCALE).astype(jnp.bfloat16)


def block_size():
    return 512


def attend(query_head, key_head, value_head, weight_two, gain_vector):
    length = query_head.shape[0]
    block_rows = block_size()
    score_scale = query_head.shape[-1] ** (-0.5)
    offsets = jnp.arange(block_rows, dtype=jnp.int32)
    value_size = value_head.shape[-1]

    def one_block(number):
        first_row = number * block_rows
        query_block = lax.dynamic_slice_in_dim(query_head, first_row, block_rows, 0)
        query_positions = first_row + offsets

        def fill_scores(kblock, buffer):
            key_block = lax.dynamic_slice_in_dim(key_head, kblock * block_rows, block_rows, 0)
            scores = (
                jnp.einsum(
                    "qcd,kcd->cqk", query_block, key_block, preferred_element_type=jnp.float32
                )
                * score_scale
            )
            visible = (kblock * block_rows + offsets)[None, :] <= query_positions[:, None]
            scores = jnp.where(visible[None], scores, -1e30)
            return lax.dynamic_update_slice_in_dim(buffer, scores, kblock * block_rows, 2)

        start_buffer = jnp.full((2, block_rows, length), -1e30, jnp.float32)
        stored = lax.fori_loop(0, number + 1, fill_scores, start_buffer)
        highest = jnp.max(stored, axis=-1)
        totals = jnp.sum(jnp.exp(stored - highest[..., None]), axis=-1)

        def weigh_values(kblock, accumulated):
            scores = lax.dynamic_slice_in_dim(stored, kblock * block_rows, block_rows, 2)
            probabilities = jnp.exp(scores - highest[..., None]) / totals[..., None]
            mixing = (probabilities[0] - weight_two * probabilities[1]).astype(jnp.bfloat16)
            value_block = lax.dynamic_slice_in_dim(value_head, kblock * block_rows, block_rows, 0)
            return accumulated + jnp.dot(mixing, value_block, preferred_element_type=jnp.float32)

        return lax.fori_loop(
            0, number + 1, weigh_values, jnp.zeros((block_rows, value_size), jnp.float32)
        )

    blocks = lax.map(one_block, jnp.arange(length // block_rows, dtype=jnp.int32))
    return head_norm(blocks.reshape(length, value_size), gain_vector)


def local(query_rows, key_rows, value_rows, query_gain, key_gain, lambdas, head_gain, out_weight):
    tok_count = query_rows.shape[1]
    group_size = lax.axis_size("sp")
    head_size = query_gain.shape[0]
    value_size = head_gain.shape[0]
    heads_total = lambdas.shape[0]
    local_heads = heads_total // group_size

    def by_peer(tensor):
        return tensor.reshape(1, tok_count, group_size, tensor.shape[2] // group_size)

    query_in, key_in, value_in = (
        lax.all_to_all(by_peer(query_rows), "sp", split_axis=2, concat_axis=1, tiled=True),
        lax.all_to_all(by_peer(key_rows), "sp", split_axis=2, concat_axis=1, tiled=True),
        lax.all_to_all(by_peer(value_rows), "sp", split_axis=2, concat_axis=1, tiled=True),
    )
    length = tok_count * group_size
    positions = jnp.arange(length, dtype=jnp.float32)
    query_rot = norm_rotate(
        query_in.reshape(length, local_heads, 2, head_size), query_gain, positions
    )
    key_rot = norm_rotate(key_in.reshape(length, local_heads, 2, head_size), key_gain, positions)
    value_heads = value_in.reshape(length, local_heads, value_size)
    local_lambdas = lax.dynamic_slice_in_dim(
        lambdas, lax.axis_index("sp") * local_heads, local_heads
    )

    def per_head(head_index):
        return attend(
            query_rot[:, head_index],
            key_rot[:, head_index],
            value_heads[:, head_index],
            local_lambdas[head_index],
            head_gain,
        )

    outputs = lax.map(per_head, jnp.arange(local_heads, dtype=jnp.int32))
    outputs = jnp.transpose(outputs, (1, 0, 2)).reshape(1, length, 1, local_heads * value_size)
    returned = lax.all_to_all(outputs, "sp", split_axis=1, concat_axis=2, tiled=True)
    heads_rows = returned.reshape(tok_count, heads_total * value_size)
    attended = jnp.dot(
        heads_rows,
        lax.all_gather(out_weight, "dp", axis=1, tiled=True),
        preferred_element_type=jnp.float32,
    )
    return attended.astype(jnp.bfloat16).reshape(1, tok_count, attended.shape[1])


def solution(mesh):
    placed = (
        P(("grp", "dp"), "sp", None),
        P(("grp", "dp"), "sp", None),
        P(("grp", "dp"), "sp", None),
        P(),
        P(),
        P(),
        P(),
        P(None, "dp"),
    )
    return jax.shard_map(
        local, mesh=mesh, in_specs=placed, out_specs=P(("grp", "dp"), "sp", None), check_vma=False
    )
```

profile of v0, /device:TPU:0, one launch (start us, length us, event | category | flops | bytes accessed | tf_op | source)
XLA Modules:
  0.0 130.4 jit_solution(3775947803156317788)
XLA Ops:
  6.5 0.7 all-gather.2.cloned.1.call-update
  7.3 0.3 copy-done.1
  7.6 1.0 copy.25
  8.6 6.3 %all-to-all-start = ((bf16[1,128,4,512]{1,3,0,2:T(8,128)(2,1)}), bf16[1,128,4,512]{1,3,0,2:T(8,128)(2,1)S(1)}, u32[]{:S(2)}, u32[]{:S(2)}) async-start(bf16[1,128,4,512]{1,3,0,2:T(8,128)(2,1)} %bitcast.7), calls=%async_computation | async-start | bytes 1048576 | tf_op jit(solution)/shard_map/all_to_all | solution.py:102
  15.0 1.0 copy.27
  16.0 13.5 %all-to-all-done = bf16[1,128,4,512]{1,3,0,2:T(8,128)(2,1)S(1)} async-done(((bf16[1,128,4,512]{1,3,0,2:T(8,128)(2,1)}), bf16[1,128,4,512]{1,3,0,2:T(8,128)(2,1)S(1)}, u32[]{:S(2)}, u32[]{:S(2)}) %all-to-all-start) | async-done | bytes 524320 | tf_op jit(solution)/shard_map/all_to_all | solution.py:102
  29.5 3.6 %all-to-all-start.1 = ((bf16[1,128,4,512]{1,3,0,2:T(8,128)(2,1)}), bf16[1,128,4,512]{1,3,0,2:T(8,128)(2,1)S(1)}, u32[]{:S(2)}, u32[]{:S(2)}) async-start(bf16[1,128,4,512]{1,3,0,2:T(8,128)(2,1)} %bitcast.10), calls=%async_computation.1 | async-start | bytes 1048576 | tf_op jit(solution)/shard_map/all_to_all | solution.py:101
  33.1 0.3 copy.29
  33.4 1.1 copy.30
  34.4 12.7 %all-to-all-done.1 = bf16[1,128,4,512]{1,3,0,2:T(8,128)(2,1)S(1)} async-done(((bf16[1,128,4,512]{1,3,0,2:T(8,128)(2,1)}), bf16[1,128,4,512]{1,3,0,2:T(8,128)(2,1)S(1)}, u32[]{:S(2)}, u32[]{:S(2)}) %all-to-all-start.1) | async-done | bytes 524320 | tf_op jit(solution)/shard_map/all_to_all | solution.py:101
  47.1 4.1 %all-to-all-start.2 = ((bf16[1,128,4,512]{3,1,0,2:T(8,128)(2,1)}), bf16[1,128,4,512]{3,1,0,2:T(8,128)(2,1)}, u32[]{:S(2)}, u32[]{:S(2)}) async-start(bf16[1,128,4,512]{3,1,0,2:T(8,128)(2,1)} %copy.30), calls=%async_computation.2 | async-start | bytes 1048576 | tf_op jit(solution)/shard_map/all_to_all | solution.py:103
  51.3 0.3 fusion.40
  51.7 0.7 copy.26
  52.4 0.4 reshape.151
  52.9 0.7 copy.28
  53.6 0.4 reshape.152
  54.0 11.3 %all-to-all-done.2 = bf16[1,128,4,512]{3,1,0,2:T(8,128)(2,1)} async-done(((bf16[1,128,4,512]{3,1,0,2:T(8,128)(2,1)}), bf16[1,128,4,512]{3,1,0,2:T(8,128)(2,1)}, u32[]{:S(2)}, u32[]{:S(2)}) %all-to-all-start.2) | async-done | bytes 524320 | tf_op jit(solution)/shard_map/all_to_all | solution.py:103
  65.3 1.2 reshape.147
  67.0 0.3 multiply_multiply_fusion.1
  67.5 0.3 subtract_convert_fusion
  67.9 1.1 pad_maximum_fusion
  69.0 26.1 %while.54 = (s32[]{:T(128)}, bf16[4,512,128]{1,2,0:T(8,128)(2,1)S(1)}, s32[4]{0:T(128)S(1)}, bf16[512,4,2,64]{0,3,2,1:T(8,128)(2,1)}, bf16[512,4,2,64]{0,3,2,1:T...) while((s32[]{:T(128)}, ...), condition=%wide.region_8.9_spmd, body=%wide.region_2.8_spmd.sunk | while | flops 138281984 | bytes 9979571 | solution.py:125
  69.0 0.6 dynamic_slice.79
  71.6 2.0 %fusion.54 = (f32[2,512]{1,0:T(2,128)S(1)}, f32[2,512,512]{1,2,0:T(8,128)S(1)}) fusion(pred[512,512]{0,1:T(8,128)(4,1)S(1)} %iota_compare_fusion.2, bf16[512,4,2,64]{0,3,2,1:T(8,128)(2,1)} %get-tuple-element.419, s32[]{:T(128)S(6)} %select_n.36, bf16[512,4,2,64]{0,3,2,1:T(8,128)(2,1)} %get-tuple-element.420), kind=kOutput, calls=%fused_computation.57.clone.1 | convolution fusion | flops 69206528 | bytes 2626560 | tf_op jit(solution)/shard_map/while/body/eval_jaxpr/while/body/eval_jaxpr/sub | solution.py:72
  73.6 0.3 broadcast_divide_fusion.2
  73.9 0.6 dynamic_slice.80
  74.4 0.9 multiply_reduce_fusion.4
  75.5 0.6 dynamic_slice.79
  78.1 2.0 %fusion.54 = (f32[2,512]{1,0:T(2,128)S(1)}, f32[2,512,512]{1,2,0:T(8,128)S(1)}) fusion(pred[512,512]{0,1:T(8,128)(4,1)S(1)} %iota_compare_fusion.2, bf16[512,4,2,64]{0,3,2,1:T(8,128)(2,1)} %get-tuple-element.419, s32[]{:T(128)S(6)} %select_n.36, bf16[512,4,2,64]{0,3,2,1:T(8,128)(2,1)} %get-tuple-element.420), kind=kOutput, calls=%fused_computation.57.clone.1 | convolution fusion | flops 69206528 | bytes 2626560 | tf_op jit(solution)/shard_map/while/body/eval_jaxpr/while/body/eval_jaxpr/sub | solution.py:72
  80.1 0.3 broadcast_divide_fusion.2
  80.4 0.6 dynamic_slice.80
  81.0 0.9 multiply_reduce_fusion.4
  82.0 0.6 dynamic_slice.79
  84.7 2.0 %fusion.54 = (f32[2,512]{1,0:T(2,128)S(1)}, f32[2,512,512]{1,2,0:T(8,128)S(1)}) fusion(pred[512,512]{0,1:T(8,128)(4,1)S(1)} %iota_compare_fusion.2, bf16[512,4,2,64]{0,3,2,1:T(8,128)(2,1)} %get-tuple-element.419, s32[]{:T(128)S(6)} %select_n.36, bf16[512,4,2,64]{0,3,2,1:T(8,128)(2,1)} %get-tuple-element.420), kind=kOutput, calls=%fused_computation.57.clone.1 | convolution fusion | flops 69206528 | bytes 2626560 | tf_op jit(solution)/shard_map/while/body/eval_jaxpr/while/body/eval_jaxpr/sub | solution.py:72
  86.9 0.6 dynamic_slice.80
  87.5 0.9 multiply_reduce_fusion.4
  88.6 0.6 dynamic_slice.79
  91.2 2.0 %fusion.54 = (f32[2,512]{1,0:T(2,128)S(1)}, f32[2,512,512]{1,2,0:T(8,128)S(1)}) fusion(pred[512,512]{0,1:T(8,128)(4,1)S(1)} %iota_compare_fusion.2, bf16[512,4,2,64]{0,3,2,1:T(8,128)(2,1)} %get-tuple-element.419, s32[]{:T(128)S(6)} %select_n.36, bf16[512,4,2,64]{0,3,2,1:T(8,128)(2,1)} %get-tuple-element.420), kind=kOutput, calls=%fused_computation.57.clone.1 | convolution fusion | flops 69206528 | bytes 2626560 | tf_op jit(solution)/shard_map/while/body/eval_jaxpr/while/body/eval_jaxpr/sub | solution.py:72
  93.4 0.6 dynamic_slice.80
  94.0 0.9 multiply_reduce_fusion.4
  95.1 0.9 copy.32
  96.0 0.5 broadcast.175
  96.5 3.8 %reduce = bf16[512,512]{1,0:T(8,128)(2,1)S(1)} reduce(bf16[512,1,1,512]{3,2,1,0:T(2,128)(2,1)S(1)} %bitcast.87, bf16[]{:T(256)} %broadcast.175), dimensions={1,2}, to_apply=%bitcast.59.reduce_sub_computation | reduce | bytes 1048578
  100.3 0.4 reshape.155
  100.7 16.4 %all_to_all.48 = bf16[4,2,32768]{2,1,0:T(2,128)(2,1)S(1)} all-to-all(bf16[4,2,32768]{2,1,0:T(2,128)(2,1)S(1)} %reshape.155), channel_id=1, replica_groups=mesh['grp'=2,'sp'=4,'dp'=4] {'sp'}, dimensions={0} | all-to-all | bytes 1048576 | tf_op jit(solution)/shard_map/all_to_all | solution.py:127
  117.1 0.5 reshape.156
  117.8 0.3 copy.33
  118.1 5.5 %fusion.38 = bf16[1,128,2048]{2,1,0:T(8,128)(2,1)} fusion(bf16[128,2048]{0,1:T(8,128)(2,1)S(1)} %bitcast.85, bf16[2048,2048]{1,0:T(8,128)(2,1)} %all-gather.2.cloned.1.call-done), kind=kOutput, calls=%fused_computation.38 | convolution fusion | flops 1074003968 | bytes 9437184 | tf_op jit(solution)/shard_map/dot_general | solution.py:129
  (44 shorter events, 2.4 us)
Async XLA Ops:
  6.5 1.0 copy-start.1
  6.5 8.4 %copy-start.2 = (bf16[1,128,2048]{2,1,0:T(8,128)(2,1)S(1)}, bf16[1,128,2048]{2,1,0:T(8,128)(2,1)}, u32[]{:S(2)}) copy-start(bf16[1,128,2048]{2,1,0:T(8,128)(2,1)} %param.12) | copy-start | bytes 1572868
  6.5 111.5 %all-gather.2.cloned.1.call-start = ((), (), s32[]{:S(2)}) async-start(), calls=%async_computation.4 | async-start | bytes 10485760 | tf_op jit(solution)/shard_map/all_gather | solution.py:131
  7.6 25.5 %copy-start.3 = (bf16[1,128,2048]{2,1,0:T(8,128)(2,1)S(1)}, bf16[1,128,2048]{2,1,0:T(8,128)(2,1)}, u32[]{:S(2)}) copy-start(bf16[1,128,2048]{2,1,0:T(8,128)(2,1)} %param.14) | copy-start | bytes 1572868
  8.6 20.8 %all-to-all-start = ((bf16[1,128,4,512]{1,3,0,2:T(8,128)(2,1)}), bf16[1,128,4,512]{1,3,0,2:T(8,128)(2,1)S(1)}, u32[]{:S(2)}, u32[]{:S(2)}) async-start(bf16[1,128,4,512]{1,3,0,2:T(8,128)(2,1)} %bitcast.7), calls=%async_computation | async-start | bytes 1048576 | tf_op jit(solution)/shard_map/all_to_all | solution.py:102
  29.5 21.8 %copy-start.7 = (f32[16]{0:T(128)S(1)}, f32[16]{0:T(128)}, u32[]{:S(2)}) copy-start(f32[16]{0:T(128)} %param.17) | copy-start | bytes 196
  29.5 17.6 %all-to-all-start.1 = ((bf16[1,128,4,512]{1,3,0,2:T(8,128)(2,1)}), bf16[1,128,4,512]{1,3,0,2:T(8,128)(2,1)S(1)}, u32[]{:S(2)}, u32[]{:S(2)}) async-start(bf16[1,128,4,512]{1,3,0,2:T(8,128)(2,1)} %bitcast.10), calls=%async_computation.1 | async-start | bytes 1048576 | tf_op jit(solution)/shard_map/all_to_all | solution.py:101
  47.1 18.2 %all-to-all-start.2 = ((bf16[1,128,4,512]{3,1,0,2:T(8,128)(2,1)}), bf16[1,128,4,512]{3,1,0,2:T(8,128)(2,1)}, u32[]{:S(2)}, u32[]{:S(2)}) async-start(bf16[1,128,4,512]{3,1,0,2:T(8,128)(2,1)} %copy.30), calls=%async_computation.2 | async-start | bytes 1048576 | tf_op jit(solution)/shard_map/all_to_all | solution.py:103
  65.3 1.6 %copy-start.5 = (f32[64]{0:T(128)S(1)}, f32[64]{0:T(128)}, u32[]{:S(2)}) copy-start(f32[64]{0:T(128)} %param.16) | copy-start | bytes 772
  66.6 0.7 copy-start.6
  67.5 1.5 %copy-start = (bf16[4,512,128]{1,2,0:T(8,128)(2,1)S(1)}, bf16[4,512,128]{1,2,0:T(8,128)(2,1)}, u32[]{:S(2)}) copy-start(bf16[4,512,128]{1,2,0:T(8,128)(2,1)} %custom-call) | copy-start | bytes 1572868
  67.5 1.5 %copy-start.4 = (f32[128]{0:T(128)S(1)}, f32[128]{0:T(128)}, u32[]{:S(2)}) copy-start(f32[128]{0:T(128)} %param.18) | copy-start | bytes 1540
Sparse Core Ops, SparseCore 0:
  8.9 60.9 all-gather.1
where the time goes:
time: 131 us; the launch traced here: 130 us
  waiting for transfers between devices  38.2 us (29%)
  matrix products  17.1 us (13%)
  blocking collectives  16.4 us (13%)
  local copies, waits for them, and re-layouts  14.6 us (11%)
  starting transfers between devices  14.1 us (11%)
  between operations  13.6 us (10%)
  other arithmetic  8.36 us (6%)
  loops' own time  7.96 us (6%)
    all_to_all x1, blocking collectives, local(): lax.all_to_all(outputs, 'sp', split_axis=1, concat_axis=2, tiled=True)  16.4 us
    all_to_all x1, waiting for transfers between devices, local(): lax.all_to_all(by_peer(key_rows), 'sp', split_axis=2, concat_axis=1, tile...  13.5 us
    all_to_all x1, waiting for transfers between devices, local(): lax.all_to_all(by_peer(query_rows), 'sp', split_axis=2, concat_axis=1, ti...  12.7 us
    all_to_all x1, waiting for transfers between devices, local(): lax.all_to_all(by_peer(value_rows), 'sp', split_axis=2, concat_axis=1, ti...  11.3 us
    another operation x1, loops' own time, local(): outputs = lax.map(per_head, jnp.arange(local_heads, dtype=jnp.int32))  7.96 us
    sub x4, matrix products, one_block(): totals = jnp.sum(jnp.exp(stored - highest[..., None]), axis=-1)  7.85 us
    all_to_all x1, starting transfers between devices, local(): lax.all_to_all(by_peer(key_rows), 'sp', split_axis=2, concat_axis=1, tile...  6.35 us
    dot_general x1, matrix products, local(): jnp.dot(heads_rows, lax.all_gather(out_weight, 'dp', axis=1, tiled=True),...  5.46 us
  transfers between devices with their start and end apart: 4, of which 3 were waited for; matrix products, arithmetic and copies ran while one was open for 26% of the time, Pallas kernels for 0%

commit v1 on v0

--- a/solution.py
+++ b/solution.py
@@ -124,7 +124,10 @@
 
     outputs = lax.map(per_head, jnp.arange(local_heads, dtype=jnp.int32))
     outputs = jnp.transpose(outputs, (1, 0, 2)).reshape(1, length, 1, local_heads * value_size)
-    returned = lax.all_to_all(outputs, "sp", split_axis=1, concat_axis=2, tiled=True)
+    returned = jnp.concatenate(
+        lax.all_to_all(jnp.stack(jnp.split(outputs, lax.axis_size("sp"), axis=1)), "sp", 0, 0),
+        axis=2,
+    )
     heads_rows = returned.reshape(tok_count, heads_total * value_size)
     attended = jnp.dot(
         heads_rows,

time: 131 us -> 125 us (0.954)
  other arithmetic: 8.36 us -> 4.63 us
  local copies, waits for them, and re-layouts: 14.6 us -> 12.1 us
    unnamed x1 -> x0, other arithmetic: 3.82 us -> none
    unnamed x23 -> x19, local copies, waits for them, and re-layouts: 4.21 us -> 2.69 us
  transfers between devices with their start and end apart: 4 -> 4, of which waited for: 3 -> 3; matrix products, arithmetic and copies ran while one was open for 26% -> 23% of each run, Pallas kernels for 0% -> 0%
where the time goes in v1:
time: 125 us; the launch traced here: 124 us
  waiting for transfers between devices  38.2 us (31%)
  matrix products  17.1 us (14%)
  blocking collectives  16.4 us (13%)
  starting transfers between devices  14.1 us (11%)
  between operations  13.6 us (11%)
  local copies, waits for them, and re-layouts  12.1 us (10%)
  loops' own time  7.96 us (6%)
  other arithmetic  4.63 us (4%)
    all_to_all x1, blocking collectives, local(): lax.all_to_all(jnp.stack(jnp.split(outputs, lax.axis_size('sp'), axis=1))...  16.4 us
    all_to_all x1, waiting for transfers between devices, local(): lax.all_to_all(by_peer(key_rows), 'sp', split_axis=2, concat_axis=1, tile...  13.5 us
    all_to_all x1, waiting for transfers between devices, local(): lax.all_to_all(by_peer(query_rows), 'sp', split_axis=2, concat_axis=1, ti...  12.7 us
    all_to_all x1, waiting for transfers between devices, local(): lax.all_to_all(by_peer(value_rows), 'sp', split_axis=2, concat_axis=1, ti...  11.3 us
    another operation x1, loops' own time, local(): outputs = lax.map(per_head, jnp.arange(local_heads, dtype=jnp.int32))  7.96 us
    sub x4, matrix products, one_block(): totals = jnp.sum(jnp.exp(stored - highest[..., None]), axis=-1)  7.85 us
    all_to_all x1, starting transfers between devices, local(): lax.all_to_all(by_peer(key_rows), 'sp', split_axis=2, concat_axis=1, tile...  6.35 us
    dot_general x1, matrix products, local(): jnp.dot(heads_rows, lax.all_gather(out_weight, 'dp', axis=1, tiled=True),...  5.46 us
  transfers between devices with their start and end apart: 4, of which 3 were waited for; matrix products, arithmetic and copies ran while one was open for 23% of the time, Pallas kernels for 0%

profile of v1, /device:TPU:0, one launch (start us, length us, event | category | flops | bytes accessed | tf_op | source)
XLA Modules:
  0.0 124.0 jit_solution(939778945097915328)
XLA Ops:
  6.5 0.7 all-gather.2.cloned.1.call-update
  7.3 0.3 copy-done
  7.6 1.0 copy.21
  8.6 6.3 %all-to-all-start = ((bf16[1,128,4,512]{1,3,0,2:T(8,128)(2,1)}), bf16[1,128,4,512]{1,3,0,2:T(8,128)(2,1)S(1)}, u32[]{:S(2)}, u32[]{:S(2)}) async-start(bf16[1,128,4,512]{1,3,0,2:T(8,128)(2,1)} %bitcast.7), calls=%async_computation | async-start | bytes 1048576 | tf_op jit(solution)/shard_map/all_to_all | solution.py:102
  15.0 1.0 copy.23
  16.0 13.5 %all-to-all-done = bf16[1,128,4,512]{1,3,0,2:T(8,128)(2,1)S(1)} async-done(((bf16[1,128,4,512]{1,3,0,2:T(8,128)(2,1)}), bf16[1,128,4,512]{1,3,0,2:T(8,128)(2,1)S(1)}, u32[]{:S(2)}, u32[]{:S(2)}) %all-to-all-start) | async-done | bytes 524320 | tf_op jit(solution)/shard_map/all_to_all | solution.py:102
  29.5 3.6 %all-to-all-start.1 = ((bf16[1,128,4,512]{1,3,0,2:T(8,128)(2,1)}), bf16[1,128,4,512]{1,3,0,2:T(8,128)(2,1)S(1)}, u32[]{:S(2)}, u32[]{:S(2)}) async-start(bf16[1,128,4,512]{1,3,0,2:T(8,128)(2,1)} %bitcast.10), calls=%async_computation.1 | async-start | bytes 1048576 | tf_op jit(solution)/shard_map/all_to_all | solution.py:101
  33.1 0.3 copy.25
  33.4 1.1 copy.26
  34.4 12.7 %all-to-all-done.1 = bf16[1,128,4,512]{1,3,0,2:T(8,128)(2,1)S(1)} async-done(((bf16[1,128,4,512]{1,3,0,2:T(8,128)(2,1)}), bf16[1,128,4,512]{1,3,0,2:T(8,128)(2,1)S(1)}, u32[]{:S(2)}, u32[]{:S(2)}) %all-to-all-start.1) | async-done | bytes 524320 | tf_op jit(solution)/shard_map/all_to_all | solution.py:101
  47.1 4.2 %all-to-all-start.2 = ((bf16[1,128,4,512]{3,1,0,2:T(8,128)(2,1)}), bf16[1,128,4,512]{3,1,0,2:T(8,128)(2,1)}, u32[]{:S(2)}, u32[]{:S(2)}) async-start(bf16[1,128,4,512]{3,1,0,2:T(8,128)(2,1)} %copy.26), calls=%async_computation.2 | async-start | bytes 1048576 | tf_op jit(solution)/shard_map/all_to_all | solution.py:103
  51.4 0.3 fusion.40
  51.8 0.7 copy.22
  52.5 0.4 reshape.150
  53.0 0.7 copy.24
  53.6 0.4 reshape.151
  54.1 11.3 %all-to-all-done.2 = bf16[1,128,4,512]{3,1,0,2:T(8,128)(2,1)} async-done(((bf16[1,128,4,512]{3,1,0,2:T(8,128)(2,1)}), bf16[1,128,4,512]{3,1,0,2:T(8,128)(2,1)}, u32[]{:S(2)}, u32[]{:S(2)}) %all-to-all-start.2) | async-done | bytes 524320 | tf_op jit(solution)/shard_map/all_to_all | solution.py:103
  65.4 1.2 reshape.146
  66.6 0.1 multiply_reduce_fusion.2
  66.8 0.1 multiply_reduce_fusion.1
  67.0 0.3 multiply_multiply_fusion.1
  67.3 0.3 multiply_multiply_fusion
  67.6 0.3 subtract_convert_fusion
  67.9 1.1 pad_maximum_fusion
  69.0 26.1 %while.54 = (s32[]{:T(128)}, bf16[4,512,128]{1,2,0:T(8,128)(2,1)S(1)}, s32[4]{0:T(128)S(1)}, bf16[512,4,2,64]{0,3,2,1:T(8,128)(2,1)}, bf16[512,4,2,64]{0,3,2,1:T...) while((s32[]{:T(128)}, ...), condition=%wide.region_8.9_spmd, body=%wide.region_2.8_spmd.sunk | while | flops 138281984 | bytes 9979571 | solution.py:125
  69.1 0.6 dynamic_slice.79
  71.7 2.0 %fusion.54 = (f32[2,512]{1,0:T(2,128)S(1)}, f32[2,512,512]{1,2,0:T(8,128)S(1)}) fusion(pred[512,512]{0,1:T(8,128)(4,1)S(1)} %iota_compare_fusion.2, bf16[512,4,2,64]{0,3,2,1:T(8,128)(2,1)} %get-tuple-element.423, s32[]{:T(128)S(6)} %select_n.36, bf16[512,4,2,64]{0,3,2,1:T(8,128)(2,1)} %get-tuple-element.424), kind=kOutput, calls=%fused_computation.62.clone.1 | convolution fusion | flops 69206528 | bytes 2626560 | tf_op jit(solution)/shard_map/while/body/eval_jaxpr/while/body/eval_jaxpr/sub | solution.py:72
  73.6 0.3 broadcast_divide_fusion.2
  73.9 0.6 dynamic_slice.80
  74.5 0.9 multiply_reduce_fusion.4
  75.5 0.1 fusion.55
  75.6 0.6 dynamic_slice.79
  78.2 2.0 %fusion.54 = (f32[2,512]{1,0:T(2,128)S(1)}, f32[2,512,512]{1,2,0:T(8,128)S(1)}) fusion(pred[512,512]{0,1:T(8,128)(4,1)S(1)} %iota_compare_fusion.2, bf16[512,4,2,64]{0,3,2,1:T(8,128)(2,1)} %get-tuple-element.423, s32[]{:T(128)S(6)} %select_n.36, bf16[512,4,2,64]{0,3,2,1:T(8,128)(2,1)} %get-tuple-element.424), kind=kOutput, calls=%fused_computation.62.clone.1 | convolution fusion | flops 69206528 | bytes 2626560 | tf_op jit(solution)/shard_map/while/body/eval_jaxpr/while/body/eval_jaxpr/sub | solution.py:72
  80.1 0.3 broadcast_divide_fusion.2
  80.4 0.6 dynamic_slice.80
  81.0 0.9 multiply_reduce_fusion.4
  82.1 0.6 dynamic_slice.79
  84.7 2.0 %fusion.54 = (f32[2,512]{1,0:T(2,128)S(1)}, f32[2,512,512]{1,2,0:T(8,128)S(1)}) fusion(pred[512,512]{0,1:T(8,128)(4,1)S(1)} %iota_compare_fusion.2, bf16[512,4,2,64]{0,3,2,1:T(8,128)(2,1)} %get-tuple-element.423, s32[]{:T(128)S(6)} %select_n.36, bf16[512,4,2,64]{0,3,2,1:T(8,128)(2,1)} %get-tuple-element.424), kind=kOutput, calls=%fused_computation.62.clone.1 | convolution fusion | flops 69206528 | bytes 2626560 | tf_op jit(solution)/shard_map/while/body/eval_jaxpr/while/body/eval_jaxpr/sub | solution.py:72
  86.7 0.3 broadcast_divide_fusion.2
  86.9 0.6 dynamic_slice.80
  87.5 0.9 multiply_reduce_fusion.4
  88.6 0.6 dynamic_slice.79
  91.2 2.0 %fusion.54 = (f32[2,512]{1,0:T(2,128)S(1)}, f32[2,512,512]{1,2,0:T(8,128)S(1)}) fusion(pred[512,512]{0,1:T(8,128)(4,1)S(1)} %iota_compare_fusion.2, bf16[512,4,2,64]{0,3,2,1:T(8,128)(2,1)} %get-tuple-element.423, s32[]{:T(128)S(6)} %select_n.36, bf16[512,4,2,64]{0,3,2,1:T(8,128)(2,1)} %get-tuple-element.424), kind=kOutput, calls=%fused_computation.62.clone.1 | convolution fusion | flops 69206528 | bytes 2626560 | tf_op jit(solution)/shard_map/while/body/eval_jaxpr/while/body/eval_jaxpr/sub | solution.py:72
  93.2 0.3 broadcast_divide_fusion.2
  93.5 0.6 dynamic_slice.80
  94.0 0.9 multiply_reduce_fusion.4
  95.3 16.4 %all_to_all.38 = bf16[4,1,128,1,512]{2,4,3,1,0:T(8,128)(2,1)S(1)} all-to-all(bf16[4,1,128,1,512]{2,4,3,1,0:T(8,128)(2,1)S(1)} %pad_maximum_fusion.2), channel_id=1, replica_groups=mesh['grp'=2,'sp'=4,'dp'=4] {'sp'}, dimensions={0} | all-to-all | bytes 1048576 | tf_op jit(solution)/shard_map/all_to_all | solution.py:128
  111.7 5.5 %fusion.38 = bf16[1,128,2048]{2,1,0:T(8,128)(2,1)} fusion(bf16[128,2048]{0,1:T(8,128)(2,1)S(1)} %bitcast.90, bf16[2048,2048]{1,0:T(8,128)(2,1)} %all-gather.2.cloned.1.call-done), kind=kOutput, calls=%fused_computation.38 | convolution fusion | flops 1074003968 | bytes 9437184 | tf_op jit(solution)/shard_map/dot_general | solution.py:132
  (39 shorter events, 1.2 us)
Async XLA Ops:
  6.5 1.0 copy-start
  6.5 8.4 %copy-start.1 = (bf16[1,128,2048]{2,1,0:T(8,128)(2,1)S(1)}, bf16[1,128,2048]{2,1,0:T(8,128)(2,1)}, u32[]{:S(2)}) copy-start(bf16[1,128,2048]{2,1,0:T(8,128)(2,1)} %param.12) | copy-start | bytes 1572868
  6.5 105.2 %all-gather.2.cloned.1.call-start = ((), (), s32[]{:S(2)}) async-start(), calls=%async_computation.4 | async-start | bytes 10485760 | tf_op jit(solution)/shard_map/all_gather | solution.py:134
  7.6 25.5 %copy-start.2 = (bf16[1,128,2048]{2,1,0:T(8,128)(2,1)S(1)}, bf16[1,128,2048]{2,1,0:T(8,128)(2,1)}, u32[]{:S(2)}) copy-start(bf16[1,128,2048]{2,1,0:T(8,128)(2,1)} %param.14) | copy-start | bytes 1572868
  8.6 20.8 %all-to-all-start = ((bf16[1,128,4,512]{1,3,0,2:T(8,128)(2,1)}), bf16[1,128,4,512]{1,3,0,2:T(8,128)(2,1)S(1)}, u32[]{:S(2)}, u32[]{:S(2)}) async-start(bf16[1,128,4,512]{1,3,0,2:T(8,128)(2,1)} %bitcast.7), calls=%async_computation | async-start | bytes 1048576 | tf_op jit(solution)/shard_map/all_to_all | solution.py:102
  29.5 21.8 %copy-start.7 = (f32[16]{0:T(128)S(1)}, f32[16]{0:T(128)}, u32[]{:S(2)}) copy-start(f32[16]{0:T(128)} %param.17) | copy-start | bytes 196
  29.5 17.6 %all-to-all-start.1 = ((bf16[1,128,4,512]{1,3,0,2:T(8,128)(2,1)}), bf16[1,128,4,512]{1,3,0,2:T(8,128)(2,1)S(1)}, u32[]{:S(2)}, u32[]{:S(2)}) async-start(bf16[1,128,4,512]{1,3,0,2:T(8,128)(2,1)} %bitcast.10), calls=%async_computation.1 | async-start | bytes 1048576 | tf_op jit(solution)/shard_map/all_to_all | solution.py:101
  47.1 18.3 %all-to-all-start.2 = ((bf16[1,128,4,512]{3,1,0,2:T(8,128)(2,1)}), bf16[1,128,4,512]{3,1,0,2:T(8,128)(2,1)}, u32[]{:S(2)}, u32[]{:S(2)}) async-start(bf16[1,128,4,512]{3,1,0,2:T(8,128)(2,1)} %copy.26), calls=%async_computation.2 | async-start | bytes 1048576 | tf_op jit(solution)/shard_map/all_to_all | solution.py:103
  65.4 1.6 %copy-start.5 = (f32[64]{0:T(128)S(1)}, f32[64]{0:T(128)}, u32[]{:S(2)}) copy-start(f32[64]{0:T(128)} %param.16) | copy-start | bytes 772
  66.6 0.7 copy-start.6
  67.6 1.5 %copy-start.3 = (bf16[4,512,128]{1,2,0:T(8,128)(2,1)S(1)}, bf16[4,512,128]{1,2,0:T(8,128)(2,1)}, u32[]{:S(2)}) copy-start(bf16[4,512,128]{1,2,0:T(8,128)(2,1)} %custom-call) | copy-start | bytes 1572868
  67.6 1.5 %copy-start.4 = (f32[128]{0:T(128)S(1)}, f32[128]{0:T(128)}, u32[]{:S(2)}) copy-start(f32[128]{0:T(128)} %param.18) | copy-start | bytes 1540
Sparse Core Ops, SparseCore 0:
  8.9 60.9 all-gather.1
